TPU v7x, 768 devices: a whole 4x8x12 slice. The times are simulated.
768 devices in a mesh: sp: 24 (over z, core), tp: 32 (over y, x).
Axes of the slice: x: 4, y: 8, z: 12, core: 2. Of those that a mesh axis runs over, the one named last changes fastest.
Arguments:
- context_activations: bfloat16 [2, 6144, 4096], P(None, 'sp', 'tp'), may hold values from -6 to 6
- first_generated_activation: bfloat16 [2, 4096], replicated, may hold values from -6 to 6
- address_projection: bfloat16 [4096, 4096], P(None, 'tp'), may hold values from -0.09375 to 0.09375
- payload_projection: bfloat16 [4096, 4096], P(None, 'tp'), may hold values from -0.09375 to 0.09375
- lookup_projection: bfloat16 [4096, 4096], P(None, 'tp'), may hold values from -0.09375 to 0.09375
- exit_gating_projection: bfloat16 [4096, 4096], P(None, 'tp'), may hold values from -0.09375 to 0.09375
- writing_intensity_projection: bfloat16 [4096, 32], replicated, may hold values from -0.09375 to 0.09375
- fading_projection: bfloat16 [4096, 32], replicated, may hold values from -0.09375 to 0.09375
- channel_fading_speed: float32 [32], replicated, may hold values from 0 to 1, as said below
- extra_fading_log: float32 [2, 6144, 32], P(None, 'sp', 'tp'), may hold values from -1 to 0, as said below
- readout_normalizer_gain: float32 [128], replicated, may hold values from 0.1 to 1.9
- exit_projection: bfloat16 [4096, 4096], P('tp'), may hold values from -0.09375 to 0.09375
Outputs:
- state_cache: bfloat16 [2, 24, 32, 128, 128], P(None, 'sp', 'tp')
- step_out: bfloat16 [2, 4096], P(None, 'tp')
Inputs may be any that keep to these rules, and one draw needn't show every extreme that they name: `channel_fading_speed`: positive rates, one a head. `extra_fading_log`: zero at all but a few positions of each prompt and head, negative there.
All inputs are finite; a program needn't handle non-finite values.
Results may differ from a plain program's by a relative error of at most 0.012.
Values may be sent and summed in bfloat16 or wider, within the bound.
A program may use at most 64 MiB of HBM per device.

v0:
```python
import jax
import jax.numpy as jnp
from jax import lax
from jax.sharding import Mesh
from jax.sharding import PartitionSpec as P

BLOCK = 64
TP = ("tp_0", "tp_1")
SP = ("sp_0", "sp_1")


norm_eps = 1e-06
highest = lax.Precision.HIGHEST


def gathered_by_axis(value, axes, dim):
    for axis in reversed(axes):
        value = lax.all_gather(value, axis, axis=dim, tiled=True)
    return value


def neutral_like(value, identity):
    return jax.tree.map(
        lambda part, zero: jnp.zeros_like(part) + jnp.asarray(zero, part.dtype), value, identity
    )


def carried_in(value, axes, combine, identity):
    before = start = neutral_like(value, identity)
    subtotal = value
    for axis in reversed(axes):
        devices, position = (lax.axis_size(axis), lax.axis_index(axis))
        pieces = jax.tree.map(
            lambda part, kind: lax.all_gather(part.astype(kind), axis),
            subtotal,
            (jnp.bfloat16, jnp.bfloat16),
        )
        inside, subtotal = (start, start)
        for k in range(devices):
            passed = k < position
            subtotal = combine(
                subtotal, jax.tree.map(lambda part, own: part[k].astype(own.dtype), pieces, value)
            )
            inside = jax.tree.map(lambda new, old: jnp.where(passed, new, old), subtotal, inside)
        before = combine(inside, before)
    return before


def prefix_by_axis(value, axes, combine, identity):
    before = start = neutral_like(value, identity)
    subtotal = value
    for axis in reversed(axes):
        devices, position = (lax.axis_size(axis), lax.axis_index(axis))
        pieces = lax.all_gather(subtotal, axis)
        inside, subtotal = (start, start)
        for k in reversed(range(devices)):
            passed = k > position
            subtotal = combine(subtotal, pieces[k])
            inside = jnp.where(passed, subtotal, inside)
        before = combine(inside, before)
    return before


def copy_for_each(value, axis):
    devices = lax.axis_size(axis)
    return lax.all_to_all(
        jnp.broadcast_to(value[None], (devices, *value.shape)), axis, 0, 0, tiled=True
    )


def of_everyone(value, axis):
    everything = copy_for_each(value, axis)
    return jnp.sum(everything, axis=0)


def cut_along(value, dim, devices):
    before, after = (value.shape[:dim], value.shape[dim + 1 :])
    return jnp.moveaxis(value.reshape(*before, devices, -1, *after), dim, 0)


def sum_at_owner(value, axis, dim):
    devices = lax.axis_size(axis)
    parts = lax.all_to_all(cut_along(value, dim, devices), axis, 0, 0, tiled=True)
    return jnp.sum(parts, axis=0)


def unit_rows(values_in):
    return values_in * lax.rsqrt(jnp.sum(values_in * values_in, axis=-1, keepdims=True) + norm_eps)


def compose(left, right):
    return jnp.einsum("...ij,...jk->...ik", left, right, precision=highest)


def segment_map(keys_in, values_in, beta_gate, fading_exponent):
    blocks = keys_in.shape[0] // BLOCK
    key_blocks = keys_in.reshape(blocks, BLOCK, -1)
    value_blocks = values_in.reshape(blocks, BLOCK, -1)
    beta_blocks = beta_gate.reshape(blocks, BLOCK)
    cumul = jnp.cumsum(fading_exponent.reshape(blocks, BLOCK), axis=-1)
    causal = jnp.tril(jnp.ones((BLOCK, BLOCK), bool))
    strict = jnp.tril(jnp.ones((BLOCK, BLOCK), bool), -1)
    gaps_log = cumul[:, :, None] - cumul[:, None, :]
    within = jnp.where(causal, jnp.exp(jnp.where(causal, gaps_log, 0.0)), 0.0)
    keys_beta = key_blocks * beta_blocks[..., None]
    strict_part = jnp.where(
        strict, jnp.einsum("nid,njd->nij", keys_beta, key_blocks, precision=highest) * within, 0.0
    )
    targets = jnp.concatenate(
        [value_blocks * beta_blocks[..., None], keys_beta * jnp.exp(cumul)[..., None]], axis=-1
    )
    system = jnp.eye(BLOCK, dtype=jnp.float32) + strict_part
    solved = lax.linalg.triangular_solve(system, targets, left_side=True, lower=True)
    width_v = value_blocks.shape[-1]
    width_k = key_blocks.shape[-1]
    pseudo_values = solved[..., :width_v]
    decayed_keys = solved[..., width_v:]
    carried_values = jnp.concatenate(
        [jnp.zeros((blocks, BLOCK, width_k), jnp.float32), pseudo_values], axis=-1
    )
    trailing = key_blocks * jnp.exp(cumul[:, -1:] - cumul)[..., None]
    block_decay = jnp.exp(cumul[:, -1])

    def advance(memory, inputs):
        pseudo, decayed, trail_keys, shrink = inputs
        fresh_values = pseudo - jnp.dot(decayed, memory, precision=highest)
        memory = memory * shrink + jnp.dot(trail_keys.T, fresh_values, precision=highest)
        return (memory, None)

    start_map = jnp.concatenate(
        [jnp.eye(width_k, dtype=jnp.float32), jnp.zeros((width_k, width_v), jnp.float32)], axis=1
    )
    memory, _ = lax.scan(advance, start_map, (carried_values, decayed_keys, trailing, block_decay))
    return memory


def combine_maps(earlier, later):
    return (compose(later[0], earlier[0]), compose(later[0], earlier[1]) + later[1])


def body(
    context_activations,
    first_generated_activation,
    address_projection,
    payload_projection,
    lookup_projection,
    exit_gating_projection,
    writing_intensity_projection,
    fading_projection,
    channel_fading_speed,
    extra_fading_log,
    readout_normalizer_gain,
    exit_projection,
):
    head_size = readout_normalizer_gain.shape[0]
    current_heads = address_projection.shape[1] // head_size
    first_head = lax.axis_index(TP) * current_heads
    beta_cols = lax.dynamic_slice_in_dim(writing_intensity_projection, first_head, current_heads, 1)
    decay_cols = lax.dynamic_slice_in_dim(fading_projection, first_head, current_heads, 1)
    logit_weight = jnp.concatenate([beta_cols, decay_cols], axis=1)
    fading_speeds = lax.dynamic_slice_in_dim(channel_fading_speed, first_head, current_heads, 0)
    seq_count, length = (context_activations.shape[0], context_activations.shape[1])
    portion = gathered_by_axis(context_activations, TP, 2)
    key_sum = jnp.einsum(
        "abf,fc->abc", portion, address_projection, preferred_element_type=jnp.float32
    )
    value_sum = jnp.einsum(
        "abf,fc->abc", portion, payload_projection, preferred_element_type=jnp.float32
    )
    logit_sum = jnp.einsum("abf,fc->abc", portion, logit_weight, preferred_element_type=jnp.float32)
    shaped = (seq_count, length, current_heads, head_size)
    keys_here = unit_rows(jax.nn.silu(key_sum).reshape(shaped)).astype(jnp.bfloat16)
    values_here = jax.nn.silu(value_sum).reshape(shaped).astype(jnp.bfloat16)
    current_scores = logit_sum.astype(jnp.bfloat16)
    beta_gate = jax.nn.sigmoid(current_scores[..., :current_heads].astype(jnp.float32))
    fading_exponent = extra_fading_log - fading_speeds * jax.nn.softplus(
        current_scores[..., current_heads:].astype(jnp.float32)
    )
    maps = jax.vmap(jax.vmap(segment_map, in_axes=(1, 1, 1, 1)))(
        keys_here.astype(jnp.float32), values_here.astype(jnp.float32), beta_gate, fading_exponent
    )
    own_moves = maps[..., :head_size]
    own_offset = maps[..., head_size:]
    heads_shape = (seq_count, current_heads, head_size)
    new_keys = unit_rows(
        jax.nn.silu(
            jnp.dot(
                first_generated_activation, address_projection, preferred_element_type=jnp.float32
            )
        ).reshape(heads_shape)
    )
    new_values = jax.nn.silu(
        jnp.dot(first_generated_activation, payload_projection, preferred_element_type=jnp.float32)
    ).reshape(heads_shape)
    new_queries = unit_rows(
        jax.nn.silu(
            jnp.dot(
                first_generated_activation, lookup_projection, preferred_element_type=jnp.float32
            )
        ).reshape(heads_shape)
    )
    out_gate = jax.nn.silu(
        jnp.dot(
            first_generated_activation, exit_gating_projection, preferred_element_type=jnp.float32
        )
    ).reshape(heads_shape)
    new_logits = jnp.dot(
        first_generated_activation, logit_weight, preferred_element_type=jnp.float32
    )
    new_beta = jax.nn.sigmoid(new_logits[:, :current_heads])
    new_decay = jnp.exp(-fading_speeds * jax.nn.softplus(new_logits[:, current_heads:]))
    intersection_kq = jnp.sum(new_keys * new_queries, axis=-1, keepdims=True)
    carried_query = new_decay[..., None] * (
        new_queries - new_beta[..., None] * new_keys * intersection_kq
    )
    own_write = new_beta[..., None] * new_values * intersection_kq
    identity = jnp.broadcast_to(jnp.eye(head_size, dtype=jnp.float32), own_moves.shape)
    prefix_moves, prefix_offset = carried_in(
        (own_moves, own_offset), SP, combine_maps, (identity, jnp.zeros_like(own_offset))
    )
    states_here = compose(own_moves, prefix_offset) + own_offset

    def chain_later(earlier, later):
        return compose(earlier, later)

    later_moves = prefix_by_axis(own_moves, SP, chain_later, identity)
    lifted = jnp.einsum("shjk,shj->shk", later_moves, carried_query, precision=highest)
    term = jnp.einsum("shk,shkv->shv", lifted, own_offset, precision=highest)
    read = of_everyone(term, SP) + own_write
    state_cache = states_here.astype(jnp.bfloat16)[:, None]
    normed = (
        read
        * lax.rsqrt(jnp.mean(read * read, axis=-1, keepdims=True) + norm_eps)
        * readout_normalizer_gain
        * out_gate
    )
    normed = normed.astype(jnp.bfloat16).reshape(seq_count, current_heads * head_size)
    partial_out = jnp.dot(normed, exit_projection, preferred_element_type=jnp.float32)
    step_out = sum_at_owner(partial_out, TP, 1).astype(jnp.bfloat16)
    return (state_cache, step_out)


def solution(mesh):
    torus = Mesh(mesh.devices.reshape(12, 2, 8, 4), ("sp_0", "sp_1", "tp_0", "tp_1"))
    in_specs = (
        P(None, SP, TP),
        P(),
        P(None, TP),
        P(None, TP),
        P(None, TP),
        P(None, TP),
        P(),
        P(),
        P(),
        P(None, SP, TP),
        P(),
        P(TP, None),
    )
    out_specs = (P(None, SP, TP, None, None), P(None, TP))
    return jax.shard_map(body, mesh=torus, in_specs=in_specs, out_specs=out_specs, check_vma=False)
```

profile of v0, /device:TPU:1, one launch (start us, length us, event | category | flops | bytes accessed | tf_op | source)
XLA Modules:
  0.0 273.3 jit_solution(10445374709691856156)
XLA Ops:
  7.2 13.4 %all_gather.42 = bf16[2,256,512]{2,1,0:T(8,128)(2,1)} all-gather(bf16[2,256,128]{2,1,0:T(8,128)(2,1)} %param.14), channel_id=1, replica_groups=mesh['sp_0'=12,'sp_1'=2,'tp_0'=8,'tp_1'=4] {'tp_1'}, dimensions={2}, use_global_device_ids=true | all-gather | bytes 655360 | tf_op jit(solution)/shard_map/all_gather | solution.py:18
  20.8 1.2 dynamic_slice.24
  22.7 0.7 copy.87
  23.4 0.7 concatenate.12
  24.1 1.6 multiply_reduce_fusion.4
  26.3 0.9 constant_dynamic-slice_fusion.1
  27.6 62.5 %all-gather.9.cloned.1.call-done = bf16[2,256,4096]{2,1,0:T(8,128)(2,1)} async-done(((bf16[2,256,512]{2,1,0:T(8,128)(2,1)}), bf16[2,256,4096]{2,1,0:T(8,128)(2,1)}) %all-gather.9.cloned.1.call-update) | async-done | bytes 4194320 | tf_op jit(solution)/shard_map/all_gather | solution.py:18
  90.0 3.4 %fusion.17 = bf16[2,256,2]{1,2,0:T(2,128)(2,1)S(1)} fusion(bf16[2,256,4096]{2,1,0:T(8,128)(2,1)} %all-gather.9.cloned.1.call-done, bf16[4096,1]{0,1:T(2,128)(2,1)S(1)} %get-tuple-element.116, bf16[4096,1]{0,1:T(2,128)(2,1)S(1)} %get-tuple-element.117), kind=kOutput, calls=%fused_computation.41 | convolution fusion | flops 8422400 | bytes 4212736 | tf_op jit(solution)/shard_map/abf,fc->abc/dot_general | solution.py:170
  93.4 0.7 fusion.97
  95.0 3.5 %multiply_reduce_fusion = (f32[2,256]{1,0:T(2,128)S(1)}, f32[2,256,128]{2,1,0:T(8,128)S(1)}) fusion(bf16[2,256,4096]{2,1,0:T(8,128)(2,1)} %all-gather.9.cloned.1.call-done, bf16[4096,128]{1,0:T(8,128)(2,1)S(1)} %copy-done), kind=kOutput, calls=%fused_computation.60 | convolution fusion | flops 537263616 | bytes 5507072 | tf_op jit(solution)/shard_map/abf,fc->abc/dot_general | solution.py:164
  99.1 39.3 %custom-call.3 = f32[2,1,4,1,64,64]{4,5,3,2,1,0:T(8,128)S(1)} custom-call(f32[2,1,4,1,64,64]{5,4,3,2,1,0:T(8,128)S(1)} %fusion.12), custom_call_target="InvertDiagBlocksLowerTriangular" | custom-call | tf_op jit(solution)/shard_map/vmap(vmap())/triangular_solve | solution.py:113
  138.4 3.8 %multiply_convert_fusion = bf16[2,256,128]{2,1,0:T(8,128)(2,1)S(1)} fusion(bf16[2,256,4096]{2,1,0:T(8,128)(2,1)} %all-gather.9.cloned.1.call-done, bf16[4096,128]{1,0:T(8,128)(2,1)} %param.17), kind=kOutput, calls=%fused_computation.56 | convolution fusion | flops 537198592 | bytes 5373952 | tf_op jit(solution)/shard_map/abf,fc->abc/dot_general | solution.py:167
  143.3 0.9 broadcast_in_dim.70
  144.2 3.0 %while.10 = (s32[]{:T(128)}, f32[2,1,128,256]{3,2,0,1:T(8,128)S(1)}, f32[4,2,1]{1,2,0:T(1,128)S(1)}, f32[4,2,1,64,128]{4,3,0,1,2:T(8,128)S(1)}, f32[4,2,1,64,256...) while((s32[]{:T(128)}, f32[2,1,128,256]{3,2,0,1:T(8,128)S(1)}, ...), condition=%wide.region_3.4_spmd, body=%wide.region_2.3_spmd.sunk | while | flops 100827136 | bytes 1312357 | solution.py:133
  147.3 2.5 all-gather.4
  150.0 0.9 fusion.53
  151.0 1.9 all-gather
  152.9 1.9 all-gather.2
  155.4 26.3 %all-gather.3 = bf16[24,128,128]{2,1,0:T(8,128)(2,1)S(1)} all-gather(bf16[2,128,128]{2,1,0:T(8,128)(2,1)S(1)} %get-tuple-element.114), channel_id=5, replica_groups=mesh['sp_0'=12,'sp_1'=2,'tp_0'=8,'tp_1'=4] {'sp_0'}, dimensions={0}, use_global_device_ids=true | all-gather | bytes 851968 | tf_op jit(solution)/shard_map/all_gather | solution.py:34
  181.9 28.7 %all-gather.1 = bf16[24,128,128]{2,1,0:T(8,128)(2,1)S(1)} all-gather(bf16[2,128,128]{2,1,0:T(8,128)(2,1)S(1)} %get-tuple-element.112), channel_id=3, replica_groups=mesh['sp_0'=12,'sp_1'=2,'tp_0'=8,'tp_1'=4] {'sp_0'}, dimensions={0}, use_global_device_ids=true | all-gather | bytes 851968 | tf_op jit(solution)/shard_map/all_gather | solution.py:34
  214.1 1.3 fusion.51
  215.4 1.2 fusion.49
  216.6 1.2 fusion.47
  217.7 1.2 fusion.45
  218.9 1.2 fusion.43
  223.4 12.5 %all-to-all-start = ((f32[24,2,1,128]{3,2,1,0:T(1,128)}), f32[24,2,1,128]{3,2,1,0:T(1,128)S(1)}, u32[]{:S(2)}, u32[]{:S(2)}) async-start(f32[24,2,1,128]{3,2,1,0:T(1,128)} %broadcast_in_dim.76), calls=%async_computation | async-start | bytes 49152 | tf_op jit(solution)/shard_map/all_to_all | solution.py:66
  236.2 9.5 %all-to-all-done = f32[24,2,1,128]{3,2,1,0:T(1,128)S(1)} async-done(((f32[24,2,1,128]{3,2,1,0:T(1,128)}), f32[24,2,1,128]{3,2,1,0:T(1,128)S(1)}, u32[]{:S(2)}, u32[]{:S(2)}) %all-to-all-start) | async-done | bytes 24608 | tf_op jit(solution)/shard_map/all_to_all | solution.py:66
  245.7 1.6 multiply_reduce_fusion.1
  247.3 2.4 convolution_bitcast_fusion.3
  249.8 7.4 %all-to-all-start.1 = ((f32[32,2,128]{2,1,0:T(2,128)}), f32[32,2,128]{2,1,0:T(2,128)S(1)}, u32[]{:S(2)}, u32[]{:S(2)}) async-start(f32[32,2,128]{2,1,0:T(2,128)} %convolution_bitcast_fusion.3), calls=%async_computation.1 | async-start | bytes 65536 | tf_op jit(solution)/shard_map/all_to_all | solution.py:83
  257.2 0.9 fusion.16
  258.1 7.8 %all-to-all-done.1 = f32[32,2,128]{2,1,0:T(2,128)S(1)} async-done(((f32[32,2,128]{2,1,0:T(2,128)}), f32[32,2,128]{2,1,0:T(2,128)S(1)}, u32[]{:S(2)}, u32[]{:S(2)}) %all-to-all-start.1) | async-done | bytes 32800 | tf_op jit(solution)/shard_map/all_to_all | solution.py:83
  (91 shorter events, 15.0 us)
Async XLA Ops:
  7.2 18.5 %copy-start = (bf16[4096,128]{1,0:T(8,128)(2,1)S(1)}, bf16[4096,128]{1,0:T(8,128)(2,1)}, u32[]{:S(2)}) copy-start(bf16[4096,128]{1,0:T(8,128)(2,1)} %param.16) | copy-start | bytes 3145732
  7.2 15.5 %copy-start.3 = (bf16[128,4096]{1,0:T(8,128)(2,1)S(1)}, bf16[128,4096]{1,0:T(8,128)(2,1)}, u32[]{:S(2)}) copy-start(bf16[128,4096]{1,0:T(8,128)(2,1)} %param.25) | copy-start | bytes 3145732
  7.2 82.8 %all-gather.9.cloned.1.call-start = ((), (), s32[]{:S(2)}) async-start(), calls=%async_computation.2 | async-start | bytes 4718592 | tf_op jit(solution)/shard_map/all_gather | solution.py:18
  20.7 3.4 %copy-start.4 = (bf16[2,4096]{1,0:T(2,128)(2,1)S(1)}, bf16[2,4096]{1,0:T(2,128)(2,1)}, u32[]{:S(2)}) copy-start(bf16[2,4096]{1,0:T(2,128)(2,1)} %param.15) | copy-start | bytes 49156
  20.7 193.4 %all-gather.11.cloned.1.call-start = ((), (), s32[]{:S(2)}) async-start(), calls=%async_computation.3 | async-start | bytes 1703936 | tf_op jit(solution)/shard_map/all_gather | solution.py:54
  27.5 65.8 %copy-start.5 = (f32[2,256,1]{1,2,0:T(1,128)S(1)}, f32[2,256,1]{1,2,0:T(1,128)}, u32[]{:S(2)}) copy-start(f32[2,256,1]{1,2,0:T(1,128)} %param.23) | copy-start | bytes 6148
  212.7 1.0 copy-start.2
  214.1 6.0 %copy-start.1 = (f32[24,128,128]{2,1,0:T(8,128)S(1)}, f32[24,128,128]{2,1,0:T(8,128)}, u32[]{:S(2)}) copy-start(f32[24,128,128]{2,1,0:T(8,128)} %all-gather.11.cloned.1.call-done) | copy-start | bytes 4718596
  222.0 25.3 %copy-start.6 = (f32[128]{0:T(128)S(1)}, f32[128]{0:T(128)}, u32[]{:S(2)}) copy-start(f32[128]{0:T(128)} %param.24) | copy-start | bytes 1540
  223.4 22.3 %all-to-all-start = ((f32[24,2,1,128]{3,2,1,0:T(1,128)}), f32[24,2,1,128]{3,2,1,0:T(1,128)S(1)}, u32[]{:S(2)}, u32[]{:S(2)}) async-start(f32[24,2,1,128]{3,2,1,0:T(1,128)} %broadcast_in_dim.76), calls=%async_computation | async-start | bytes 49152 | tf_op jit(solution)/shard_map/all_to_all | solution.py:66
  249.8 16.1 %all-to-all-start.1 = ((f32[32,2,128]{2,1,0:T(2,128)}), f32[32,2,128]{2,1,0:T(2,128)S(1)}, u32[]{:S(2)}, u32[]{:S(2)}) async-start(f32[32,2,128]{2,1,0:T(2,128)} %convolution_bitcast_fusion.3), calls=%async_computation.1 | async-start | bytes 65536 | tf_op jit(solution)/shard_map/all_to_all | solution.py:83
Sparse Core Ops, SparseCore 0:
  20.8 69.1 all-gather.8
  151.1 52.9 all-gather.10
where the time goes:
time: 274 us; the launch traced here: 273 us
  waiting for transfers between devices  79.8 us (29%)
  blocking collectives  74.7 us (27%)
  other arithmetic  42 us (15%)
  matrix products  35.8 us (13%)
  starting transfers between devices  20 us (7%)
  between operations  15.3 us (6%)
  local copies, waits for them, and re-layouts  5.64 us (2%)
    all_gather x1, waiting for transfers between devices, gathered_by_axis(): value = lax.all_gather(value, axis, axis=dim, tiled=True)  62.5 us
    all_gather x4, blocking collectives, carried_in(): lax.all_gather(part.astype(kind), axis)  58.8 us
    another operation x1, other arithmetic, segment_map(): lax.linalg.triangular_solve(system, targets, left_side=True, lower=True)  39.3 us
    dot_general x36, matrix products, compose(): return jnp.einsum('...ij,...jk->...ik', left, right, precision=highest)  14.6 us
    all_gather x1, blocking collectives, gathered_by_axis(): value = lax.all_gather(value, axis, axis=dim, tiled=True)  13.4 us
    all_to_all x1, starting transfers between devices, copy_for_each(): lax.all_to_all(jnp.broadcast_to(value[None], (devices, *value.shape)), ax...  12.5 us
    all_to_all x1, waiting for transfers between devices, copy_for_each(): lax.all_to_all(jnp.broadcast_to(value[None], (devices, *value.shape)), ax...  9.5 us
    all_to_all x1, waiting for transfers between devices, sum_at_owner(): lax.all_to_all(cut_along(value, dim, devices), axis, 0, 0, tiled=True)  7.8 us
  transfers between devices with their start and end apart: 4, of which 3 were waited for; matrix products, arithmetic and copies ran while one was open for 4% of the time, Pallas kernels for 0%

commit v1 on v0

v1 whole, which is shorter than its diff:
```python
import jax
import jax.numpy as jnp
from jax import lax
from jax.experimental import pallas as pl
from jax.experimental.pallas import tpu as pltpu
from jax.sharding import Mesh
from jax.sharding import PartitionSpec as P

NZ, NC, NY, NX = 12, 2, 8, 4
NT = NY * NX
HEAD = 128
RUN = 256
ROWS = 2 * RUN
WIDTH = NT * 128
KEEP = NX * 128
PIECES = 4
UP, DOWN = 6, 5
MESH = pl.DeviceIdType.MESH
f32, bf16 = jnp.float32, jnp.bfloat16
norm_eps = 1e-06

A = (0, 192)
A_HALF = ((0, 96), (96, 96))
B = (192, 320)
B_HALF = ((192, 160), (352, 160))


def dot(a, b):
    return jnp.dot(a, b, preferred_element_type=f32)


def dot_nt(a, b):
    return lax.dot_general(a, b, (((1,), (1,)), ((), ())), preferred_element_type=f32)


def split(a):
    high = a.astype(bf16)
    return high, (a - high.astype(f32)).astype(bf16)


def wide_left(a):
    high, low = split(a)
    return jnp.concatenate([high, low], axis=1)


def dot_ff(a, b):
    high, low = split(b)
    both = jnp.concatenate([high, low], axis=1)
    out = dot(wide_left(a), jnp.concatenate([both, both], axis=0))
    return out[:, :128] + out[:, 128:]


def dot_fb(a, b):
    return dot(wide_left(a), jnp.concatenate([b, b], axis=0))


def dot_bf(a, b):
    high, low = split(b)
    return dot(jnp.concatenate([a, a], axis=1), jnp.concatenate([high, low], axis=0))


def silu(v):
    return v / (1.0 + jnp.exp(-v))


def sigmoid(v):
    return 1.0 / (1.0 + jnp.exp(-v))


def softplus(v):
    return jnp.maximum(v, 0.0) + jnp.log1p(jnp.exp(-jnp.abs(v)))


def unit(v):
    return v * lax.rsqrt(jnp.sum(v * v, axis=-1, keepdims=True) + norm_eps)


def iota(shape, dim):
    return lax.broadcasted_iota(jnp.int32, shape, dim)


def inverses(systems):
    row, col = iota((128, 128), 0), iota((128, 128), 1)
    eye = (row == col).astype(f32)

    def lower_blocks(bits):
        r, c = row >> bits, col >> bits
        return (r == c + 1) & ((r & 1) == 1)

    found = [eye - jnp.where(lower_blocks(0), a, 0.0) for a in systems]
    for bits in range(1, 7):
        chosen = lower_blocks(bits)
        right = [dot_ff(jnp.where(chosen, a, 0.0), t) for a, t in zip(systems, found)]
        found = [t - dot_ff(t, r) for t, r in zip(found, right)]
    return found


def run_maps(keys, values, beta_logits, decay_logits, extra_rows, speed):
    row, col = iota((RUN, RUN), 0), iota((RUN, RUN), 1)
    causal = row >= col
    systems, trails, betas, grown, lasts = [], [], [], [], []
    for p in range(2):
        beta_col = sigmoid(beta_logits[p])
        pace_col = softplus(decay_logits[p])
        pace_row = jnp.sum(jnp.where(row == col, pace_col, 0.0), axis=0, keepdims=True)
        fade_row = extra_rows[p] - speed * pace_row
        cum_col = jnp.sum(jnp.where(causal, fade_row, 0.0), axis=1, keepdims=True)
        cum_row = jnp.sum(jnp.where(row == col, cum_col, 0.0), axis=0, keepdims=True)
        beta_row = jnp.sum(jnp.where(row == col, beta_col, 0.0), axis=0, keepdims=True)
        last = cum_row[:, RUN - 1 :]
        within = jnp.where(causal, jnp.exp(jnp.where(causal, cum_col - cum_row, 0.0)), 0.0)
        gram = dot_nt(keys[p], keys[p])
        systems.append(jnp.where(row > col, gram * within * beta_col, 0.0))
        trails.append(keys[p].astype(f32).T * jnp.exp(last - cum_row))
        betas.append(beta_row)
        grown.append(jnp.exp(cum_row))
        lasts.append(jnp.exp(last))
    solved = inverses([systems[0][:128, :128], systems[0][128:, 128:],
                       systems[1][:128, :128], systems[1][128:, 128:]])
    maps = []
    diagonal = iota((128, 128), 0) == iota((128, 128), 1)
    for p in range(2):
        second = dot_ff(trails[p][:, 128:], solved[2 * p + 1])
        first = trails[p][:, :128] - dot_ff(second, systems[p][128:, :128])
        first = dot_ff(first, solved[2 * p])
        writes = jnp.concatenate([first, second], axis=1) * betas[p]
        offset = dot_fb(writes, values[p])
        moves = jnp.where(diagonal, lasts[p], 0.0) - dot_fb(writes * grown[p], keys[p])
        maps.append(jnp.concatenate([moves, offset], axis=1))
    return maps


def kernel(
    x_hbm, fg_hbm, wk_hbm, wv_hbm, wq_hbm, wz_hbm, wb_hbm, wd_hbm, speeds, extra_hbm, gain_hbm, wo_hbm,
    cache_ref, step_ref,
    chunks, wkv, wqz, wlogit, wl, wo, fg, extra, gain,
    acc, acc_l, facc, own_map, other_map, blocks, state_out, state_in, parts_out, parts_in, row_out, row_in,
    load_sem, gather_send, ax_sem, ay_sem, by_sem, bx_sem,
    swap_send, swap_recv, ring_send, up_sem, down_sem, part_send, part_recv,
):
    z, c = lax.axis_index("z"), lax.axis_index("c")
    y, x = lax.axis_index("y"), lax.axis_index("x")
    mine = y * NX + x

    def ring(at, step, size):
        return lax.rem(at + (step % size), size)

    def slot(yy, xx):
        return yy * NX + xx

    def load(src, dst, sem):
        copy = pltpu.make_async_copy(src, dst, load_sem.at[sem])
        copy.start()
        return copy

    own_load = load(x_hbm, chunks.at[mine], 0)
    logit_loads = [
        load(wb_hbm, wlogit.at[pl.ds(0, 32)], 1),
        load(wd_hbm, wlogit.at[pl.ds(32, 32)], 2),
    ]
    early_loads = [
        load(fg_hbm, fg, 3),
        load(wk_hbm, wkv.at[:, pl.ds(0, 128)], 4),
        load(wv_hbm, wkv.at[:, pl.ds(128, 128)], 5),
        load(wq_hbm, wqz.at[:, pl.ds(0, 128)], 6),
        load(wz_hbm, wqz.at[:, pl.ds(128, 128)], 7),
    ]
    late_loads = [load(extra_hbm, extra, 8), load(gain_hbm, gain, 9), load(wo_hbm, wo, 10)]

    barrier = pltpu.get_barrier_semaphore()

    def greet(d, carry):
        other = lax.rem(mine + d, NT)
        pl.semaphore_signal(
            barrier, inc=1, device_id={"y": other // NX, "x": lax.rem(other, NX)}, device_id_type=MESH
        )
        return carry

    lax.fori_loop(1, NT, greet, 0)
    pl.semaphore_signal(barrier, inc=1, device_id={"z": ring(z, 1, NZ)}, device_id_type=MESH)
    pl.semaphore_signal(barrier, inc=1, device_id={"z": ring(z, -1, NZ)}, device_id_type=MESH)
    pl.semaphore_signal(barrier, inc=1, device_id={"c": 1 - c}, device_id_type=MESH)

    for copy in logit_loads:
        copy.wait()
    pick_row, pick_col = iota((16, 64), 0), iota((16, 64), 1)
    pick = ((pick_row == 0) & (pick_col == mine)) | ((pick_row == 1) & (pick_col == mine + 32))
    wl[...] = dot(jnp.where(pick, 1.0, 0.0).astype(bf16), wlogit[...]).astype(bf16)
    own_load.wait()
    pl.semaphore_wait(barrier, NT - 1 + 3)

    y_to = ({"y": ring(y, 1, NY)}, {"y": ring(y, -1, NY)})
    x_to = ({"x": ring(x, 1, NX)}, {"x": ring(x, -1, NX)})
    sign = (-1, 1)

    def chunk_copy(yy, xx, rows, sem, to):
        view = chunks.at[slot(yy, xx), pl.ds(rows[0], rows[1])]
        return pltpu.make_async_remote_copy(
            src_ref=view, dst_ref=view, send_sem=gather_send, recv_sem=sem, device_id=to, device_id_type=MESH
        )

    def ax(k, h, start):
        xx = ring(x, sign[k] * (h - 1 if start else h), NX)
        copy = chunk_copy(y, xx, A if h < 2 else A_HALF[k], ax_sem.at[k, h - 1], x_to[k])
        copy.start() if start else copy.wait_recv()

    def ay(k, h, j, start):
        yy = ring(y, sign[k] * (h - 1 if start else h), NY)
        copy = chunk_copy(yy, ring(x, j, NX), A if h < 4 else A_HALF[k], ay_sem.at[k, h - 1, j], y_to[k])
        copy.start() if start else copy.wait_recv()

    def by(k, h, start):
        yy = ring(y, sign[k] * (h - 1 if start else h), NY)
        copy = chunk_copy(yy, x, B if h < 4 else B_HALF[k], by_sem.at[k, h - 1], y_to[k])
        copy.start() if start else copy.wait_recv()

    def bx(k, h, j, start):
        xx = ring(x, sign[k] * (h - 1 if start else h), NX)
        copy = chunk_copy(ring(y, j, NY), xx, B if h < 2 else B_HALF[k], bx_sem.at[k, h - 1, j % NY], x_to[k])
        copy.start() if start else copy.wait_recv()

    both = (0, 1)

    def project(steps):
        def one(yy):
            row = pl.multiple_of(yy * KEEP, KEEP)
            left = jnp.concatenate([chunks[yy * NX + i] for i in range(NX)], axis=1)
            acc[...] += dot(left, wkv[pl.ds(row, KEEP), :])
            acc_l[...] += dot_nt(left, wl[:, pl.ds(row, KEEP)])

        for step in steps:
            one(ring(y, step, NY))

    def bx_first(j):
        for k in both:
            bx(k, 1, j, False)
            bx(k, 2, j, True)

    def bx_last(j):
        for k in both:
            bx(k, 2, j, False)

    def ay_pass(h, j):
        for k in both:
            ay(k, h, j, False)
            if h < 4:
                ay(k, h + 1, j, True)

    def by_pass(h):
        for k in both:
            by(k, h, False)
            if h < 4:
                by(k, h + 1, True)
        for j in (-h, h) if h < 4 else (4,):
            for k in both:
                bx(k, 1, j, True)

    for k in both:
        by(k, 1, True)
        ax(k, 1, True)
    for k in both:
        bx(k, 1, 0, True)
        ay(k, 1, 0, True)

    for copy in early_loads:
        copy.wait()
    facc[...] = jnp.zeros_like(facc)
    acc[...] = jnp.zeros_like(acc)
    acc_l[...] = jnp.zeros_like(acc_l)

    def first_step(i, carry):
        at = pl.multiple_of(i * KEEP, KEEP)
        left = fg[:, pl.ds(at, KEEP)]
        facc[:, 0:256] += dot(left, wkv[pl.ds(at, KEEP), :])
        facc[:, 256:512] += dot(left, wqz[pl.ds(at, KEEP), :])
        facc[:, 512:528] += dot_nt(left, wl[:, pl.ds(at, KEEP)])
        return carry

    lax.fori_loop(0, WIDTH // KEEP, first_step, 0)

    for k in both:
        ax(k, 1, False)
        ax(k, 2, True)
    for k in both:
        ay(k, 1, 1, True)
        ay(k, 1, 3, True)
    by_pass(1)
    bx_first(0)
    ay_pass(1, 0)
    for k in both:
        ax(k, 2, False)
    for k in both:
        ay(k, 1, 2, True)
    by_pass(2)
    ay_pass(1, 1)
    ay_pass(1, 3)
    bx_first(-1)
    bx_first(1)
    bx_last(0)
    ay_pass(1, 2)
    by_pass(3)
    ay_pass(2, 0)
    ay_pass(2, 1)
    project([0])
    ay_pass(2, 3)
    bx_first(-2)
    bx_first(2)
    bx_last(-1)
    bx_last(1)
    ay_pass(2, 2)
    by_pass(4)
    ay_pass(3, 0)
    project([-1])
    ay_pass(3, 1)
    ay_pass(3, 3)
    bx_first(-3)
    bx_first(3)
    project([1])
    ay_pass(3, 2)
    bx_last(-2)
    bx_last(2)
    bx_first(4)
    project([-2, 2])
    bx_last(-3)
    bx_last(3)
    project([-3, 3])
    for j in range(NX):
        ay_pass(4, j)
    bx_last(4)
    project([4])

    for copy in late_loads:
        copy.wait()
    speed = speeds[mine]
    keys = unit(silu(acc[:, 0:128])).astype(bf16)
    values = silu(acc[:, 128:256]).astype(bf16)
    logits = acc_l[...].astype(bf16).astype(f32)
    maps = run_maps(
        [keys[:RUN], keys[RUN:]],
        [values[:RUN], values[RUN:]],
        [logits[:RUN, 0:1], logits[RUN:, 0:1]],
        [logits[:RUN, 1:2], logits[RUN:, 1:2]],
        [extra[0], extra[1]],
        speed,
    )

    own_map[0] = maps[0]
    own_map[1] = maps[1]

    def swap(src, dst, i):
        return pltpu.make_async_remote_copy(
            src_ref=src, dst_ref=dst, send_sem=swap_send.at[i], recv_sem=swap_recv.at[i],
            device_id={"c": 1 - c}, device_id_type=MESH,
        )

    map_swap = swap(own_map.at[1 - c], other_map, 0)
    map_swap.start()

    my_row = iota((2, 1), 0) == c

    def chosen(lo, hi):
        return jnp.sum(jnp.where(my_row, facc[:, lo:hi], 0.0), axis=0, keepdims=True)

    new_key = unit(silu(chosen(0, 128)))
    new_value = silu(chosen(128, 256))
    new_query = unit(silu(chosen(256, 384)))
    out_gate = silu(chosen(384, 512))
    new_beta = sigmoid(chosen(512, 513))
    new_decay = jnp.exp(-speed * softplus(chosen(513, 514)))
    meeting = jnp.sum(new_key * new_query, axis=-1, keepdims=True)
    carried_query = new_decay * (new_query - new_beta * new_key * meeting)
    own_write = new_beta * new_value * meeting

    map_swap.wait()
    here = jnp.where(c == 0, maps[0], maps[1])
    there = other_map[...]
    early = jnp.where(c == 0, here, there)
    late = jnp.where(c == 0, there, here)
    zeros = jnp.zeros((128, 128), f32)

    def with_offset(product, offset):
        return jnp.concatenate([product[:, :128], product[:, 128:] + offset], axis=1)

    pair = jnp.concatenate(
        [dot_ff(late[:, :128], early[:, :128]), dot_ff(late[:, :128], early[:, 128:]) + late[:, 128:]], axis=1
    )
    blocks[z] = pair.astype(bf16)

    z_to = ({"z": ring(z, 1, NZ)}, {"z": ring(z, -1, NZ)})
    piece_rows = 128 // PIECES
    z_sem = (up_sem, down_sem)

    def hop(k, h, q, start):
        zz = ring(z, sign[k] * (h - 1 if start else h), NZ)
        view = blocks.at[zz, pl.ds(q * piece_rows, piece_rows)]
        copy = pltpu.make_async_remote_copy(
            src_ref=view, dst_ref=view, send_sem=ring_send, recv_sem=z_sem[k].at[h - 1, q],
            device_id=z_to[k], device_id_type=MESH,
        )
        copy.start() if start else copy.wait_recv()

    limit = (UP, DOWN)
    for q in range(PIECES):
        for k in both:
            hop(k, 1, q, True)

    eye = (iota((128, 128), 0) == iota((128, 128), 1)).astype(f32)
    before = jnp.concatenate([eye, zeros], axis=1)
    reader = jnp.concatenate(
        [jnp.where(iota((8, 128), 0) == 0, carried_query, 0.0), jnp.zeros((8, 128), f32)], axis=1
    )
    after = before
    start_state = jnp.concatenate([zeros, zeros], axis=1)
    for h in range(1, UP + 1):
        for q in range(PIECES):
            for k in both:
                if h <= limit[k]:
                    hop(k, h, q, False)
                    if h < limit[k]:
                        hop(k, h + 1, q, True)
        block = blocks[ring(z, -h, NZ)]
        stacked = jnp.concatenate([before, reader], axis=0)
        grown = with_offset(dot_fb(stacked[:, :128], block), stacked[:, 128:])
        earlier = z >= h
        before = jnp.where(earlier, grown[:128], before)
        reader = jnp.where(earlier, reader, grown[128:])
        if h <= DOWN:
            block = blocks[ring(z, h, NZ)]
            later = z + h < NZ
            taken = jnp.where(later, after, start_state)
            grown = dot_bf(block[:, :128], taken)
            grown = with_offset(grown, block[:, 128:].astype(f32))
            after = jnp.where(later, grown, after)
            start_state = jnp.where(later, start_state, grown)

    entering = dot_ff(before[:, :128], start_state[:, 128:]) + before[:, 128:]
    leaving = dot_ff(jnp.concatenate([early[:, :128], pair[:, :128]], axis=0), entering)
    state_first = leaving[:128] + early[:, 128:]
    state_second = leaving[128:] + pair[:, 128:]

    state_out[...] = jnp.where(c == 0, state_second, state_first).astype(bf16)
    state_swap = swap(state_out, state_in, 1)
    state_swap.start()

    final_map = jnp.concatenate(
        [dot_ff(reader[:, :128], after[:, :128]), dot_ff(reader[:, :128], after[:, 128:])], axis=1
    )
    read = dot_ff(final_map[:, :128], state_second) + final_map[:, 128:] + reader[:, 128:]
    read = read[0:1] + own_write
    normed = read * lax.rsqrt(jnp.mean(read * read, axis=-1, keepdims=True) + norm_eps) * gain[...] * out_gate
    normed = jnp.broadcast_to(normed, (8, 128)).astype(bf16)
    partial = dot(normed, wo[...])
    for t in range(NT):
        parts_out[t] = partial[0:1, t * 128 : (t + 1) * 128]

    def part(d):
        other = lax.rem(mine + d, NT)
        return pltpu.make_async_remote_copy(
            src_ref=parts_out.at[other], dst_ref=parts_in.at[d - 1], send_sem=part_send, recv_sem=part_recv,
            device_id={"y": other // NX, "x": lax.rem(other, NX)}, device_id_type=MESH,
        )

    def send_part(d, carry):
        part(d).start()
        return carry

    lax.fori_loop(1, NT, send_part, 0)
    state_swap.wait()
    kept = jnp.where(c == 0, state_first, state_second).astype(bf16)
    came = state_in[...]
    cache_ref[0] = jnp.where(c == 0, kept, came)
    cache_ref[1] = jnp.where(c == 0, came, kept)
    total = parts_out[mine]
    pltpu.make_async_copy(parts_in, parts_in, part_recv).wait()
    total = total + jnp.sum(parts_in[...], axis=0)
    row_out[...] = total
    row_swap = swap(row_out, row_in, 2)
    row_swap.start()
    row_swap.wait()
    step_ref[...] = jnp.where(my_row, total, row_in[...]).astype(bf16)

    sent = chunks.at[pl.ds(0, NT - 1)]
    pltpu.make_async_copy(sent, sent, gather_send).wait()
    sent = blocks.at[pl.ds(0, UP + DOWN)]
    pltpu.make_async_copy(sent, sent, ring_send).wait()
    pltpu.make_async_copy(parts_in, parts_in, part_send).wait()


def body(
    context_activations,
    first_generated_activation,
    address_projection,
    payload_projection,
    lookup_projection,
    exit_gating_projection,
    writing_intensity_projection,
    fading_projection,
    channel_fading_speed,
    extra_fading_log,
    readout_normalizer_gain,
    exit_projection,
):
    hbm = pl.BlockSpec(memory_space=pl.ANY)
    vmem = pl.BlockSpec(memory_space=pltpu.VMEM)
    dma = pltpu.SemaphoreType.DMA
    cache, step = pl.pallas_call(
        kernel,
        out_shape=(jax.ShapeDtypeStruct((2, HEAD, HEAD), bf16), jax.ShapeDtypeStruct((2, 128), bf16)),
        in_specs=[hbm] * 8 + [pl.BlockSpec(memory_space=pltpu.SMEM)] + [hbm] * 3,
        out_specs=(vmem, vmem),
        scratch_shapes=[
            pltpu.VMEM((NT, ROWS, 128), bf16),
            pltpu.VMEM((WIDTH, 256), bf16),
            pltpu.VMEM((WIDTH, 256), bf16),
            pltpu.VMEM((64, WIDTH), bf16),
            pltpu.VMEM((16, WIDTH), bf16),
            pltpu.VMEM((HEAD, WIDTH), bf16),
            pltpu.VMEM((2, WIDTH), bf16),
            pltpu.VMEM((2, 1, RUN), f32),
            pltpu.VMEM((1, HEAD), f32),
            pltpu.VMEM((ROWS, 256), f32),
            pltpu.VMEM((ROWS, 16), f32),
            pltpu.VMEM((2, 528), f32),
            pltpu.VMEM((2, 128, 256), f32),
            pltpu.VMEM((128, 256), f32),
            pltpu.VMEM((NZ, 128, 256), bf16),
            pltpu.VMEM((128, 128), bf16),
            pltpu.VMEM((128, 128), bf16),
            pltpu.VMEM((NT, 1, 128), f32),
            pltpu.VMEM((NT - 1, 1, 128), f32),
            pltpu.VMEM((1, 128), f32),
            pltpu.VMEM((1, 128), f32),
            dma((11,)),
            dma,
            dma((2, 2)),
            dma((2, 4, NX)),
            dma((2, 4)),
            dma((2, 2, NY)),
            dma((3,)),
            dma((3,)),
            dma,
            dma((UP, PIECES)),
            dma((DOWN, PIECES)),
            dma,
            dma,
        ],
        compiler_params=pltpu.CompilerParams(
            collective_id=0, has_side_effects=True, vmem_limit_bytes=40 * 1024 * 1024
        ),
    )(
        context_activations.reshape(ROWS, 128),
        first_generated_activation,
        address_projection,
        payload_projection,
        lookup_projection,
        exit_gating_projection,
        writing_intensity_projection.T,
        fading_projection.T,
        channel_fading_speed,
        jnp.transpose(extra_fading_log, (0, 2, 1)),
        readout_normalizer_gain.reshape(1, HEAD),
        exit_projection,
    )
    return cache.reshape(2, 1, 1, HEAD, HEAD), step


def solution(mesh):
    torus = Mesh(mesh.devices.reshape(NZ, NC, NY, NX), ("z", "c", "y", "x"))
    SP, TP = ("z", "c"), ("y", "x")
    in_specs = (
        P(None, SP, TP),
        P(),
        P(None, TP),
        P(None, TP),
        P(None, TP),
        P(None, TP),
        P(),
        P(),
        P(),
        P(None, SP, TP),
        P(),
        P(TP, None),
    )
    out_specs = (P(None, SP, TP, None, None), P(None, TP))
    return jax.shard_map(body, mesh=torus, in_specs=in_specs, out_specs=out_specs, check_vma=False)
```

time: 274 us -> 96.9 us (0.35)
  Pallas kernels: 0 us -> 84.3 us
  waiting for transfers between devices: 79.8 us -> 0 us
  blocking collectives: 74.7 us -> 0 us
  other arithmetic: 42 us -> 0 us
  matrix products: 35.8 us -> 0 us
  starting transfers between devices: 20 us -> 0 us
  between operations: 15.3 us -> 0.68 us
  local copies, waits for them, and re-layouts: 5.64 us -> 11.4 us
    pallas_call x0 -> x1, Pallas kernels: none -> 84.3 us  [body(): pl.pallas_call(kernel, out_shape=(jax.ShapeDtypeStruct((2, HEAD, HEAD), b...]
    all_gather x6 -> x0, blocking collectives: 74.7 us -> none  [the longest x4 58.8 us: carried_in(): lax.all_gather(part.astype(kind), axis)]
    all_gather x2 -> x0, waiting for transfers between devices: 62.5 us -> none  [the longest x1 62.5 us: gathered_by_axis(): value = lax.all_gather(value, axis, axis=dim, tiled=True)]
    another operation x2 -> x0, other arithmetic: 39.8 us -> none  [the longest x1 39.3 us: segment_map(): lax.linalg.triangular_solve(system, targets, left_side=True, lower=True)]
    dot_general x55 -> x0, matrix products: 35.1 us -> none  [the longest x36 14.6 us: compose(): return jnp.einsum('...ij,...jk->...ik', left, right, precision=highest)]
    all_to_all x2 -> x0, starting transfers between devices: 19.9 us -> none  [the longest x1 12.5 us: copy_for_each(): lax.all_to_all(jnp.broadcast_to(value[None], (devices, *value.shape)), ax...]
    all_to_all x2 -> x0, waiting for transfers between devices: 17.3 us -> none  [the longest x1 9.5 us: copy_for_each(): lax.all_to_all(jnp.broadcast_to(value[None], (devices, *value.shape)), ax...]
    unnamed x14 -> x26, local copies, waits for them, and re-layouts: 0.04 us -> 11.4 us
  transfers between devices with their start and end apart: 4 -> 0, of which waited for: 3 -> 0; matrix products, arithmetic and copies ran while one was open for 4% -> 0% of each run, Pallas kernels for 0% -> 0%
where the time goes in v1:
time: 96.9 us; the launch traced here: 96.4 us
  Pallas kernels  84.3 us (87%)
  local copies, waits for them, and re-layouts  11.4 us (12%)
    pallas_call x1, Pallas kernels, body(): pl.pallas_call(kernel, out_shape=(jax.ShapeDtypeStruct((2, HEAD, HEAD), b...  84.3 us
    unnamed x26, local copies, waits for them, and re-layouts  11.4 us

profile of v1, /device:TPU:1, one launch (start us, length us, event | category | flops | bytes accessed | tf_op | source)
XLA Modules:
  0.0 96.4 jit_solution(6657509457013242111)
XLA Ops:
  0.6 0.0 copy-start.9
  0.6 0.0 copy-start.10
  0.7 0.0 copy-start.11
  0.7 0.7 copy-done.9
  1.3 0.0 copy-done.10
  1.3 0.0 copy-done.11
  1.3 0.0 copy-start
  1.3 1.2 %copy-done = bf16[4096,128]{1,0:T(8,128)(2,1)S(1)} copy-done((bf16[4096,128]{1,0:T(8,128)(2,1)S(1)}, bf16[4096,128]{1,0:T(8,128)(2,1)}, u32[]{:S(2)}) %copy-start) | copy-done | bytes 1048600
  2.5 0.0 copy-start.1
  2.6 1.2 %copy-done.1 = bf16[4096,128]{1,0:T(8,128)(2,1)S(1)} copy-done((bf16[4096,128]{1,0:T(8,128)(2,1)S(1)}, bf16[4096,128]{1,0:T(8,128)(2,1)}, u32[]{:S(2)}) %copy-start.1) | copy-done | bytes 1048600
  3.8 0.0 copy-start.2
  3.8 1.2 %copy-done.2 = bf16[4096,128]{1,0:T(8,128)(2,1)S(1)} copy-done((bf16[4096,128]{1,0:T(8,128)(2,1)S(1)}, bf16[4096,128]{1,0:T(8,128)(2,1)}, u32[]{:S(2)}) %copy-start.2) | copy-done | bytes 1048600
  5.0 0.0 copy-start.3
  5.0 1.2 %copy-done.3 = bf16[4096,128]{1,0:T(8,128)(2,1)S(1)} copy-done((bf16[4096,128]{1,0:T(8,128)(2,1)S(1)}, bf16[4096,128]{1,0:T(8,128)(2,1)}, u32[]{:S(2)}) %copy-start.3) | copy-done | bytes 1048600
  6.2 0.0 copy-start.4
  6.2 1.2 %copy-done.4 = bf16[128,4096]{1,0:T(8,128)(2,1)S(1)} copy-done((bf16[128,4096]{1,0:T(8,128)(2,1)S(1)}, bf16[128,4096]{1,0:T(8,128)(2,1)}, u32[]{:S(2)}) %copy-start.4) | copy-done | bytes 1048600
  7.5 0.0 copy-start.5
  7.5 0.9 copy-done.5
  8.4 0.0 copy-start.6
  8.4 0.9 copy-done.6
  9.4 0.0 copy-start.7
  9.4 0.9 copy-done.7
  10.3 0.0 copy-start.8
  10.3 0.7 copy-done.8
  11.0 84.3 %shard_map.131 = (bf16[2,128,128]{2,1,0:T(8,128)(2,1)S(1)}, bf16[2,128]{1,0:T(2,128)(2,1)S(1)}) custom-call(bf16[512,128]{1,0:T(8,128)(2,1)S(1)} %bitcast.10, bf16[2,4096]{1,0:T(2,128)(2,1)S(1)} %copy-done.8, bf16[4096,128]{1,0:T(8,128)(2,1)S(1)} %copy-done, bf16[4096,128]{1,0:T(8,128)(2,1)S(1)} %copy-done.1, bf16[4096,128]{1,0:T(8,128)(2,1)S(1)} %copy-done.2, ...), custom_call_target="tpu_custom_call" | custom-call | tf_op jit(solution)/shard_map/pallas_call | solution.py:506
  95.3 0.6 copy.17
  95.9 0.5 copy.18
Async XLA Ops:
  0.6 0.7 copy-start.9
  0.6 0.7 copy-start.10
  0.7 0.7 copy-start.11
  1.3 1.2 %copy-start = (bf16[4096,128]{1,0:T(8,128)(2,1)S(1)}, bf16[4096,128]{1,0:T(8,128)(2,1)}, u32[]{:S(2)}) copy-start(bf16[4096,128]{1,0:T(8,128)(2,1)} %wk_hbm.1) | copy-start | bytes 3145732
  2.5 1.2 %copy-start.1 = (bf16[4096,128]{1,0:T(8,128)(2,1)S(1)}, bf16[4096,128]{1,0:T(8,128)(2,1)}, u32[]{:S(2)}) copy-start(bf16[4096,128]{1,0:T(8,128)(2,1)} %wv_hbm.1) | copy-start | bytes 3145732
  3.8 1.2 %copy-start.2 = (bf16[4096,128]{1,0:T(8,128)(2,1)S(1)}, bf16[4096,128]{1,0:T(8,128)(2,1)}, u32[]{:S(2)}) copy-start(bf16[4096,128]{1,0:T(8,128)(2,1)} %wq_hbm.1) | copy-start | bytes 3145732
  5.0 1.2 %copy-start.3 = (bf16[4096,128]{1,0:T(8,128)(2,1)S(1)}, bf16[4096,128]{1,0:T(8,128)(2,1)}, u32[]{:S(2)}) copy-start(bf16[4096,128]{1,0:T(8,128)(2,1)} %wz_hbm.1) | copy-start | bytes 3145732
  6.2 1.2 %copy-start.4 = (bf16[128,4096]{1,0:T(8,128)(2,1)S(1)}, bf16[128,4096]{1,0:T(8,128)(2,1)}, u32[]{:S(2)}) copy-start(bf16[128,4096]{1,0:T(8,128)(2,1)} %wo_hbm.1) | copy-start | bytes 3145732
  7.5 0.9 copy-start.5
  8.4 0.9 copy-start.6
  9.4 0.9 copy-start.7
  10.3 0.7 copy-start.8

commit v2 on v1

--- a/solution.py
+++ b/solution.py
@@ -19,10 +19,10 @@
 f32, bf16 = jnp.float32, jnp.bfloat16
 norm_eps = 1e-06
 
-A = (0, 192)
-A_HALF = ((0, 96), (96, 96))
-B = (192, 320)
-B_HALF = ((192, 160), (352, 160))
+A = (0, 208)
+A_HALF = ((0, 112), (112, 96))
+B = (208, 304)
+B_HALF = ((208, 144), (352, 160))
 
 
 def dot(a, b):
@@ -131,9 +131,9 @@
 
 
 def kernel(
-    x_hbm, fg_hbm, wk_hbm, wv_hbm, wq_hbm, wz_hbm, wb_hbm, wd_hbm, speeds, extra_hbm, gain_hbm, wo_hbm,
+    x_hbm, fg_hbm, wk_hbm, wv_hbm, wq_hbm, wz_hbm, wb_hbm, wd_hbm, speed_hbm, extra_hbm, gain_hbm, wo_hbm,
     cache_ref, step_ref,
-    chunks, wkv, wqz, wlogit, wl, wo, fg, extra, gain,
+    chunks, wkv, wqz, wlogit, wl, wo, fg, extra, gain, speeds,
     acc, acc_l, facc, own_map, other_map, blocks, state_out, state_in, parts_out, parts_in, row_out, row_in,
     load_sem, gather_send, ax_sem, ay_sem, by_sem, bx_sem,
     swap_send, swap_recv, ring_send, up_sem, down_sem, part_send, part_recv,
@@ -165,29 +165,17 @@
         load(wq_hbm, wqz.at[:, pl.ds(0, 128)], 6),
         load(wz_hbm, wqz.at[:, pl.ds(128, 128)], 7),
     ]
-    late_loads = [load(extra_hbm, extra, 8), load(gain_hbm, gain, 9), load(wo_hbm, wo, 10)]
+    late_loads = [
+        load(extra_hbm, extra, 8), load(gain_hbm, gain, 9), load(wo_hbm, wo, 10), load(speed_hbm, speeds, 11)
+    ]
 
     barrier = pltpu.get_barrier_semaphore()
-
-    def greet(d, carry):
-        other = lax.rem(mine + d, NT)
-        pl.semaphore_signal(
-            barrier, inc=1, device_id={"y": other // NX, "x": lax.rem(other, NX)}, device_id_type=MESH
-        )
-        return carry
-
-    lax.fori_loop(1, NT, greet, 0)
-    pl.semaphore_signal(barrier, inc=1, device_id={"z": ring(z, 1, NZ)}, device_id_type=MESH)
-    pl.semaphore_signal(barrier, inc=1, device_id={"z": ring(z, -1, NZ)}, device_id_type=MESH)
+    for axis, at, size in (("x", x, NX), ("y", y, NY), ("z", z, NZ)):
+        for step in (1, -1):
+            pl.semaphore_signal(barrier, inc=1, device_id={axis: ring(at, step, size)}, device_id_type=MESH)
     pl.semaphore_signal(barrier, inc=1, device_id={"c": 1 - c}, device_id_type=MESH)
-
-    for copy in logit_loads:
-        copy.wait()
-    pick_row, pick_col = iota((16, 64), 0), iota((16, 64), 1)
-    pick = ((pick_row == 0) & (pick_col == mine)) | ((pick_row == 1) & (pick_col == mine + 32))
-    wl[...] = dot(jnp.where(pick, 1.0, 0.0).astype(bf16), wlogit[...]).astype(bf16)
     own_load.wait()
-    pl.semaphore_wait(barrier, NT - 1 + 3)
+    pl.semaphore_wait(barrier, 7)
 
     y_to = ({"y": ring(y, 1, NY)}, {"y": ring(y, -1, NY)})
     x_to = ({"x": ring(x, 1, NX)}, {"x": ring(x, -1, NX)})
@@ -262,8 +250,11 @@
         bx(k, 1, 0, True)
         ay(k, 1, 0, True)
 
-    for copy in early_loads:
+    for copy in logit_loads:
         copy.wait()
+    pick_row, pick_col = iota((16, 64), 0), iota((16, 64), 1)
+    pick = ((pick_row == 0) & (pick_col == mine)) | ((pick_row == 1) & (pick_col == mine + 32))
+    wl[...] = dot(jnp.where(pick, 1.0, 0.0).astype(bf16), wlogit[...]).astype(bf16)
     facc[...] = jnp.zeros_like(facc)
     acc[...] = jnp.zeros_like(acc)
     acc_l[...] = jnp.zeros_like(acc_l)
@@ -275,8 +266,6 @@
         facc[:, 256:512] += dot(left, wqz[pl.ds(at, KEEP), :])
         facc[:, 512:528] += dot_nt(left, wl[:, pl.ds(at, KEEP)])
         return carry
-
-    lax.fori_loop(0, WIDTH // KEEP, first_step, 0)
 
     for k in both:
         ax(k, 1, False)
@@ -301,6 +290,8 @@
     by_pass(3)
     ay_pass(2, 0)
     ay_pass(2, 1)
+    for copy in early_loads:
+        copy.wait()
     project([0])
     ay_pass(2, 3)
     bx_first(-2)
@@ -309,6 +300,7 @@
     bx_last(1)
     ay_pass(2, 2)
     by_pass(4)
+    lax.fori_loop(0, 4, first_step, 0)
     ay_pass(3, 0)
     project([-1])
     ay_pass(3, 1)
@@ -320,6 +312,7 @@
     bx_last(-2)
     bx_last(2)
     bx_first(4)
+    lax.fori_loop(4, 8, first_step, 0)
     project([-2, 2])
     bx_last(-3)
     bx_last(3)
@@ -331,7 +324,7 @@
 
     for copy in late_loads:
         copy.wait()
-    speed = speeds[mine]
+    speed = jnp.sum(jnp.where(iota((1, NT), 1) == mine, speeds[...], 0.0), axis=1, keepdims=True)
     keys = unit(silu(acc[:, 0:128])).astype(bf16)
     values = silu(acc[:, 128:256]).astype(bf16)
     logits = acc_l[...].astype(bf16).astype(f32)
@@ -344,146 +337,149 @@
         speed,
     )
 
-    own_map[0] = maps[0]
-    own_map[1] = maps[1]
+    other_core = {"c": 1 - c}
 
     def swap(src, dst, i):
         return pltpu.make_async_remote_copy(
             src_ref=src, dst_ref=dst, send_sem=swap_send.at[i], recv_sem=swap_recv.at[i],
-            device_id={"c": 1 - c}, device_id_type=MESH,
+            device_id=other_core, device_id_type=MESH,
         )
 
-    map_swap = swap(own_map.at[1 - c], other_map, 0)
-    map_swap.start()
-
-    my_row = iota((2, 1), 0) == c
-
-    def chosen(lo, hi):
-        return jnp.sum(jnp.where(my_row, facc[:, lo:hi], 0.0), axis=0, keepdims=True)
-
-    new_key = unit(silu(chosen(0, 128)))
-    new_value = silu(chosen(128, 256))
-    new_query = unit(silu(chosen(256, 384)))
-    out_gate = silu(chosen(384, 512))
-    new_beta = sigmoid(chosen(512, 513))
-    new_decay = jnp.exp(-speed * softplus(chosen(513, 514)))
-    meeting = jnp.sum(new_key * new_query, axis=-1, keepdims=True)
-    carried_query = new_decay * (new_query - new_beta * new_key * meeting)
-    own_write = new_beta * new_value * meeting
-
-    map_swap.wait()
-    here = jnp.where(c == 0, maps[0], maps[1])
-    there = other_map[...]
-    early = jnp.where(c == 0, here, there)
-    late = jnp.where(c == 0, there, here)
-    zeros = jnp.zeros((128, 128), f32)
-
-    def with_offset(product, offset):
-        return jnp.concatenate([product[:, :128], product[:, 128:] + offset], axis=1)
-
-    pair = jnp.concatenate(
-        [dot_ff(late[:, :128], early[:, :128]), dot_ff(late[:, :128], early[:, 128:]) + late[:, 128:]], axis=1
-    )
-    blocks[z] = pair.astype(bf16)
-
-    z_to = ({"z": ring(z, 1, NZ)}, {"z": ring(z, -1, NZ)})
-    piece_rows = 128 // PIECES
-    z_sem = (up_sem, down_sem)
-
-    def hop(k, h, q, start):
-        zz = ring(z, sign[k] * (h - 1 if start else h), NZ)
-        view = blocks.at[zz, pl.ds(q * piece_rows, piece_rows)]
-        copy = pltpu.make_async_remote_copy(
-            src_ref=view, dst_ref=view, send_sem=ring_send, recv_sem=z_sem[k].at[h - 1, q],
-            device_id=z_to[k], device_id_type=MESH,
-        )
-        copy.start() if start else copy.wait_recv()
-
-    limit = (UP, DOWN)
-    for q in range(PIECES):
-        for k in both:
-            hop(k, 1, q, True)
-
-    eye = (iota((128, 128), 0) == iota((128, 128), 1)).astype(f32)
-    before = jnp.concatenate([eye, zeros], axis=1)
-    reader = jnp.concatenate(
-        [jnp.where(iota((8, 128), 0) == 0, carried_query, 0.0), jnp.zeros((8, 128), f32)], axis=1
-    )
-    after = before
-    start_state = jnp.concatenate([zeros, zeros], axis=1)
-    for h in range(1, UP + 1):
+    both_prompts = (0, 1)
+    map_swap = swap(own_map, other_map, 0)
+    state_swap = swap(state_out, state_in, 1)
+    row_swap = swap(row_out, row_in, 2)
+
+    @pl.when(c == 0)
+    def _():
+        own_map[0] = maps[0]
+        own_map[1] = maps[1]
+        map_swap.start()
+        state_swap.wait_recv()
+        cache_ref[...] = state_in[...]
+        row_swap.wait_recv()
+        step_ref[...] = row_in[...].astype(bf16)
+        map_swap.wait_send()
+
+    @pl.when(c == 1)
+    def _():
+        first = facc[...]
+        new_key = unit(silu(first[:, 0:128]))
+        new_value = silu(first[:, 128:256])
+        new_query = unit(silu(first[:, 256:384]))
+        out_gate = silu(first[:, 384:512])
+        new_beta = sigmoid(first[:, 512:513])
+        new_decay = jnp.exp(-speed * softplus(first[:, 513:514]))
+        meeting = jnp.sum(new_key * new_query, axis=-1, keepdims=True)
+        carried_query = new_decay * (new_query - new_beta * new_key * meeting)
+        own_write = new_beta * new_value * meeting
+
+        zeros = jnp.zeros((128, 128), f32)
+        eye = (iota((128, 128), 0) == iota((128, 128), 1)).astype(f32)
+
+        def with_offset(product, offset):
+            return jnp.concatenate([product[:, :128], product[:, 128:] + offset], axis=1)
+
+        z_to = ({"z": ring(z, 1, NZ)}, {"z": ring(z, -1, NZ)})
+        z_sem = (up_sem, down_sem)
+        per_prompt = PIECES // 2
+        piece_rows = 128 // per_prompt
+
+        def hop(k, h, q, start):
+            zz = ring(z, sign[k] * (h - 1 if start else h), NZ)
+            view = blocks.at[zz, q // per_prompt, pl.ds(q % per_prompt * piece_rows, piece_rows)]
+            copy = pltpu.make_async_remote_copy(
+                src_ref=view, dst_ref=view, send_sem=ring_send, recv_sem=z_sem[k].at[h - 1, q],
+                device_id=z_to[k], device_id_type=MESH,
+            )
+            copy.start() if start else copy.wait_recv()
+
+        map_swap.wait_recv()
+        pair = []
+        for p in both_prompts:
+            early, late = other_map[p], maps[p]
+            product = [dot_ff(late[:, :128], early[:, i * 128 : (i + 1) * 128]) for i in range(2)]
+            pair.append(jnp.concatenate([product[0], product[1] + late[:, 128:]], axis=1))
+            blocks[z, p] = pair[p].astype(bf16)
         for q in range(PIECES):
             for k in both:
-                if h <= limit[k]:
-                    hop(k, h, q, False)
-                    if h < limit[k]:
-                        hop(k, h + 1, q, True)
-        block = blocks[ring(z, -h, NZ)]
-        stacked = jnp.concatenate([before, reader], axis=0)
-        grown = with_offset(dot_fb(stacked[:, :128], block), stacked[:, 128:])
-        earlier = z >= h
-        before = jnp.where(earlier, grown[:128], before)
-        reader = jnp.where(earlier, reader, grown[128:])
-        if h <= DOWN:
-            block = blocks[ring(z, h, NZ)]
-            later = z + h < NZ
-            taken = jnp.where(later, after, start_state)
-            grown = dot_bf(block[:, :128], taken)
-            grown = with_offset(grown, block[:, 128:].astype(f32))
-            after = jnp.where(later, grown, after)
-            start_state = jnp.where(later, start_state, grown)
-
-    entering = dot_ff(before[:, :128], start_state[:, 128:]) + before[:, 128:]
-    leaving = dot_ff(jnp.concatenate([early[:, :128], pair[:, :128]], axis=0), entering)
-    state_first = leaving[:128] + early[:, 128:]
-    state_second = leaving[128:] + pair[:, 128:]
-
-    state_out[...] = jnp.where(c == 0, state_second, state_first).astype(bf16)
-    state_swap = swap(state_out, state_in, 1)
-    state_swap.start()
-
-    final_map = jnp.concatenate(
-        [dot_ff(reader[:, :128], after[:, :128]), dot_ff(reader[:, :128], after[:, 128:])], axis=1
-    )
-    read = dot_ff(final_map[:, :128], state_second) + final_map[:, 128:] + reader[:, 128:]
-    read = read[0:1] + own_write
-    normed = read * lax.rsqrt(jnp.mean(read * read, axis=-1, keepdims=True) + norm_eps) * gain[...] * out_gate
-    normed = jnp.broadcast_to(normed, (8, 128)).astype(bf16)
-    partial = dot(normed, wo[...])
-    for t in range(NT):
-        parts_out[t] = partial[0:1, t * 128 : (t + 1) * 128]
-
-    def part(d):
-        other = lax.rem(mine + d, NT)
-        return pltpu.make_async_remote_copy(
-            src_ref=parts_out.at[other], dst_ref=parts_in.at[d - 1], send_sem=part_send, recv_sem=part_recv,
-            device_id={"y": other // NX, "x": lax.rem(other, NX)}, device_id_type=MESH,
-        )
-
-    def send_part(d, carry):
-        part(d).start()
-        return carry
-
-    lax.fori_loop(1, NT, send_part, 0)
-    state_swap.wait()
-    kept = jnp.where(c == 0, state_first, state_second).astype(bf16)
-    came = state_in[...]
-    cache_ref[0] = jnp.where(c == 0, kept, came)
-    cache_ref[1] = jnp.where(c == 0, came, kept)
-    total = parts_out[mine]
-    pltpu.make_async_copy(parts_in, parts_in, part_recv).wait()
-    total = total + jnp.sum(parts_in[...], axis=0)
-    row_out[...] = total
-    row_swap = swap(row_out, row_in, 2)
-    row_swap.start()
-    row_swap.wait()
-    step_ref[...] = jnp.where(my_row, total, row_in[...]).astype(bf16)
+                hop(k, 1, q, True)
+
+        limit = (UP, DOWN)
+        before = [jnp.concatenate([eye, zeros], axis=1)] * 2
+        after = [jnp.concatenate([eye, zeros], axis=1)] * 2
+        start_state = [jnp.concatenate([zeros, zeros], axis=1)] * 2
+        reader = [
+            jnp.concatenate(
+                [jnp.where(iota((8, 128), 0) == 0, carried_query[p : p + 1], 0.0), jnp.zeros((8, 128), f32)], axis=1
+            )
+            for p in both_prompts
+        ]
+        for h in range(1, UP + 1):
+            for p in both_prompts:
+                for q in range(p * per_prompt, (p + 1) * per_prompt):
+                    for k in both:
+                        if h <= limit[k]:
+                            hop(k, h, q, False)
+                            if h < limit[k]:
+                                hop(k, h + 1, q, True)
+                block = blocks[ring(z, -h, NZ), p]
+                stacked = jnp.concatenate([before[p], reader[p]], axis=0)
+                grown = with_offset(dot_fb(stacked[:, :128], block), stacked[:, 128:])
+                earlier = z >= h
+                before[p] = jnp.where(earlier, grown[:128], before[p])
+                reader[p] = jnp.where(earlier, reader[p], grown[128:])
+                if h <= DOWN:
+                    block = blocks[ring(z, h, NZ), p]
+                    later = z + h < NZ
+                    taken = jnp.where(later, after[p], start_state[p])
+                    grown = dot_bf(block[:, :128], taken)
+                    grown = with_offset(grown, block[:, 128:].astype(f32))
+                    after[p] = jnp.where(later, grown, after[p])
+                    start_state[p] = jnp.where(later, start_state[p], grown)
+
+        seconds, reads = [], []
+        for p in both_prompts:
+            entering = dot_ff(before[p][:, :128], start_state[p][:, 128:]) + before[p][:, 128:]
+            second = dot_ff(pair[p][:, :128], entering) + pair[p][:, 128:]
+            early = other_map[p]
+            state_out[p] = (dot_ff(early[:, :128], entering) + early[:, 128:]).astype(bf16)
+            tail = [dot_ff(reader[p][:, :128], after[p][:, i * 128 : (i + 1) * 128]) for i in range(2)]
+            read = dot_ff(tail[0], second) + tail[1] + reader[p][:, 128:]
+            seconds.append(second)
+            reads.append(read[0:1])
+        state_swap.start()
+        read = jnp.concatenate(reads, axis=0) + own_write
+        normed = read * lax.rsqrt(jnp.mean(read * read, axis=-1, keepdims=True) + norm_eps) * gain[...] * out_gate
+        partial = dot(normed.astype(bf16), wo[...])
+        for t in range(NT):
+            parts_out[t] = partial[:, t * 128 : (t + 1) * 128]
+
+        def send_part(d, carry):
+            other = lax.rem(mine + d, NT)
+            pltpu.make_async_remote_copy(
+                src_ref=parts_out.at[other], dst_ref=parts_in.at[d - 1], send_sem=part_send, recv_sem=part_recv,
+                device_id={"y": other // NX, "x": lax.rem(other, NX)}, device_id_type=MESH,
+            ).start()
+            return carry
+
+        lax.fori_loop(1, NT, send_part, 0)
+        for p in both_prompts:
+            cache_ref[p] = seconds[p].astype(bf16)
+        total = parts_out[mine]
+        pltpu.make_async_copy(parts_in, parts_in, part_recv).wait()
+        total = total + jnp.sum(parts_in[...], axis=0)
+        row_out[...] = total
+        row_swap.start()
+        step_ref[...] = total.astype(bf16)
+        state_swap.wait_send()
+        row_swap.wait_send()
+        sent = blocks.at[pl.ds(0, UP + DOWN)]
+        pltpu.make_async_copy(sent, sent, ring_send).wait()
+        pltpu.make_async_copy(parts_in, parts_in, part_send).wait()
 
     sent = chunks.at[pl.ds(0, NT - 1)]
     pltpu.make_async_copy(sent, sent, gather_send).wait()
-    sent = blocks.at[pl.ds(0, UP + DOWN)]
-    pltpu.make_async_copy(sent, sent, ring_send).wait()
-    pltpu.make_async_copy(parts_in, parts_in, part_send).wait()
 
 
 def body(
@@ -500,13 +496,13 @@
     readout_normalizer_gain,
     exit_projection,
 ):
-    hbm = pl.BlockSpec(memory_space=pl.ANY)
+    hbm = pl.BlockSpec(memory_space=pltpu.HBM)
     vmem = pl.BlockSpec(memory_space=pltpu.VMEM)
     dma = pltpu.SemaphoreType.DMA
     cache, step = pl.pallas_call(
         kernel,
         out_shape=(jax.ShapeDtypeStruct((2, HEAD, HEAD), bf16), jax.ShapeDtypeStruct((2, 128), bf16)),
-        in_specs=[hbm] * 8 + [pl.BlockSpec(memory_space=pltpu.SMEM)] + [hbm] * 3,
+        in_specs=[hbm] * 12,
         out_specs=(vmem, vmem),
         scratch_shapes=[
             pltpu.VMEM((NT, ROWS, 128), bf16),
@@ -518,19 +514,20 @@
             pltpu.VMEM((2, WIDTH), bf16),
             pltpu.VMEM((2, 1, RUN), f32),
             pltpu.VMEM((1, HEAD), f32),
+            pltpu.VMEM((1, NT), f32),
             pltpu.VMEM((ROWS, 256), f32),
             pltpu.VMEM((ROWS, 16), f32),
             pltpu.VMEM((2, 528), f32),
             pltpu.VMEM((2, 128, 256), f32),
-            pltpu.VMEM((128, 256), f32),
-            pltpu.VMEM((NZ, 128, 256), bf16),
-            pltpu.VMEM((128, 128), bf16),
-            pltpu.VMEM((128, 128), bf16),
-            pltpu.VMEM((NT, 1, 128), f32),
-            pltpu.VMEM((NT - 1, 1, 128), f32),
-            pltpu.VMEM((1, 128), f32),
-            pltpu.VMEM((1, 128), f32),
-            dma((11,)),
+            pltpu.VMEM((2, 128, 256), f32),
+            pltpu.VMEM((NZ, 2, 128, 256), bf16),
+            pltpu.VMEM((2, 128, 128), bf16),
+            pltpu.VMEM((2, 128, 128), bf16),
+            pltpu.VMEM((NT, 2, 128), f32),
+            pltpu.VMEM((NT - 1, 2, 128), f32),
+            pltpu.VMEM((2, 128), f32),
+            pltpu.VMEM((2, 128), f32),
+            dma((12,)),
             dma,
             dma((2, 2)),
             dma((2, 4, NX)),
@@ -545,7 +542,7 @@
             dma,
         ],
         compiler_params=pltpu.CompilerParams(
-            collective_id=0, has_side_effects=True, vmem_limit_bytes=40 * 1024 * 1024
+            collective_id=0, has_side_effects=True, vmem_limit_bytes=67_043_328
         ),
     )(
         context_activations.reshape(ROWS, 128),
@@ -556,7 +553,7 @@
         exit_gating_projection,
         writing_intensity_projection.T,
         fading_projection.T,
-        channel_fading_speed,
+        channel_fading_speed.reshape(1, NT),
         jnp.transpose(extra_fading_log, (0, 2, 1)),
         readout_normalizer_gain.reshape(1, HEAD),
         exit_projection,

time: 96.9 us -> 78.8 us (0.81)
  local copies, waits for them, and re-layouts: 11.4 us -> 1.99 us
  Pallas kernels: 84.3 us -> 76 us
    unnamed x26 -> x4, local copies, waits for them, and re-layouts: 11.4 us -> 1.99 us
    pallas_call x1, Pallas kernels: 84.3 us -> 76 us  [body(): pl.pallas_call(kernel, out_shape=(jax.ShapeDtypeStruct((2, HEAD, HEAD), b...]
where the time goes in v2:
time: 78.8 us; the launch traced here: 78.6 us
  Pallas kernels  76 us (96%)
  local copies, waits for them, and re-layouts  1.99 us (3%)
    pallas_call x1, Pallas kernels, body(): pl.pallas_call(kernel, out_shape=(jax.ShapeDtypeStruct((2, HEAD, HEAD), b...  76 us
    unnamed x4, local copies, waits for them, and re-layouts  1.99 us

profile of v2, /device:TPU:1, one launch (start us, length us, event | category | flops | bytes accessed | tf_op | source)
XLA Modules:
  0.0 78.6 jit_solution(15782709847753515954)
XLA Ops:
  0.6 76.0 %shard_map.131 = (bf16[2,128,128]{2,1,0:T(8,128)(2,1)}, bf16[2,128]{1,0:T(2,128)(2,1)}) custom-call(bf16[512,128]{1,0:T(8,128)(2,1)} %bitcast.11, bf16[2,4096]{1,0:T(2,128)(2,1)} %fg_hbm.1, bf16[4096,128]{1,0:T(8,128)(2,1)} %wk_hbm.1, bf16[4096,128]{1,0:T(8,128)(2,1)} %wv_hbm.1, bf16[4096,128]{1,0:T(8,128)(2,1)} %wq_hbm.1, bf16[4096,128]{1,0:T(8,128)(2,1)} %wz_hbm.1, ...), custom_call_target="tpu_custom_call" | custom-call | tf_op jit(solution)/shard_map/pallas_call | solution.py:502
  76.6 0.0 copy-start
  76.7 1.5 %copy.17 = bf16[2,1,1,128,128]{4,3,2,1,0:T(8,128)(2,1)} copy(bf16[2,1,1,128,128]{4,3,2,1,0:T(8,128)(2,1)} %bitcast.12) | data formatting | bytes 131072
  78.1 0.0 copy-done
  78.1 0.5 copy.18
Async XLA Ops:
  76.6 1.5 %copy-start = (bf16[2,128]{1,0:T(2,128)(2,1)S(1)}, bf16[2,128]{1,0:T(2,128)(2,1)}, u32[]{:S(2)}) copy-start(bf16[2,128]{1,0:T(2,128)(2,1)} %get-tuple-element.11) | copy-start | bytes 1540

commit v3 on v2

--- a/solution.py
+++ b/solution.py
@@ -13,7 +13,7 @@
 ROWS = 2 * RUN
 WIDTH = NT * 128
 KEEP = NX * 128
-PIECES = 4
+PIECES = 8
 UP, DOWN = 6, 5
 MESH = pl.DeviceIdType.MESH
 f32, bf16 = jnp.float32, jnp.bfloat16
@@ -271,48 +271,56 @@
         ax(k, 1, False)
         ax(k, 2, True)
     for k in both:
-        ay(k, 1, 1, True)
-        ay(k, 1, 3, True)
-    by_pass(1)
+        by(k, 1, False)
+        by(k, 2, True)
+    for j in (1, 3):
+        for k in both:
+            ay(k, 1, j, True)
+    for j in (-1, 1):
+        for k in both:
+            bx(k, 1, j, True)
     bx_first(0)
     ay_pass(1, 0)
     for k in both:
         ax(k, 2, False)
     for k in both:
         ay(k, 1, 2, True)
+    for copy in early_loads:
+        copy.wait()
+
+    @pl.when(c == 1)
+    def _():
+        lax.fori_loop(0, WIDTH // KEEP, first_step, 0)
+
     by_pass(2)
+    bx_first(-1)
     ay_pass(1, 1)
     ay_pass(1, 3)
-    bx_first(-1)
     bx_first(1)
     bx_last(0)
     ay_pass(1, 2)
     by_pass(3)
     ay_pass(2, 0)
+    project([0])
     ay_pass(2, 1)
-    for copy in early_loads:
-        copy.wait()
-    project([0])
+    bx_first(-2)
     ay_pass(2, 3)
-    bx_first(-2)
     bx_first(2)
     bx_last(-1)
     bx_last(1)
     ay_pass(2, 2)
     by_pass(4)
-    lax.fori_loop(0, 4, first_step, 0)
     ay_pass(3, 0)
+    bx_first(-3)
     project([-1])
     ay_pass(3, 1)
+    bx_first(3)
     ay_pass(3, 3)
-    bx_first(-3)
-    bx_first(3)
     project([1])
-    ay_pass(3, 2)
     bx_last(-2)
     bx_last(2)
+    ay_pass(3, 2)
     bx_first(4)
-    lax.fori_loop(4, 8, first_step, 0)
     project([-2, 2])
     bx_last(-3)
     bx_last(3)
@@ -352,8 +360,8 @@
 
     @pl.when(c == 0)
     def _():
-        own_map[0] = maps[0]
-        own_map[1] = maps[1]
+        own_map[0] = maps[0].astype(bf16)
+        own_map[1] = maps[1].astype(bf16)
         map_swap.start()
         state_swap.wait_recv()
         cache_ref[...] = state_in[...]
@@ -398,12 +406,11 @@
         pair = []
         for p in both_prompts:
             early, late = other_map[p], maps[p]
-            product = [dot_ff(late[:, :128], early[:, i * 128 : (i + 1) * 128]) for i in range(2)]
-            pair.append(jnp.concatenate([product[0], product[1] + late[:, 128:]], axis=1))
+            pair.append(with_offset(dot_fb(late[:, :128], early), late[:, 128:]))
             blocks[z, p] = pair[p].astype(bf16)
-        for q in range(PIECES):
-            for k in both:
-                hop(k, 1, q, True)
+            for q in range(p * per_prompt, (p + 1) * per_prompt):
+                for k in both:
+                    hop(k, 1, q, True)
 
         limit = (UP, DOWN)
         before = [jnp.concatenate([eye, zeros], axis=1)] * 2
@@ -416,13 +423,13 @@
             for p in both_prompts
         ]
         for h in range(1, UP + 1):
+            for q in range(PIECES):
+                for k in both:
+                    if h <= limit[k]:
+                        hop(k, h, q, False)
+                        if h < limit[k]:
+                            hop(k, h + 1, q, True)
             for p in both_prompts:
-                for q in range(p * per_prompt, (p + 1) * per_prompt):
-                    for k in both:
-                        if h <= limit[k]:
-                            hop(k, h, q, False)
-                            if h < limit[k]:
-                                hop(k, h + 1, q, True)
                 block = blocks[ring(z, -h, NZ), p]
                 stacked = jnp.concatenate([before[p], reader[p]], axis=0)
                 grown = with_offset(dot_fb(stacked[:, :128], block), stacked[:, 128:])
@@ -438,32 +445,31 @@
                     after[p] = jnp.where(later, grown, after[p])
                     start_state[p] = jnp.where(later, start_state[p], grown)
 
-        seconds, reads = [], []
+        enter, seconds, reads = [], [], []
         for p in both_prompts:
-            entering = dot_ff(before[p][:, :128], start_state[p][:, 128:]) + before[p][:, 128:]
-            second = dot_ff(pair[p][:, :128], entering) + pair[p][:, 128:]
-            early = other_map[p]
-            state_out[p] = (dot_ff(early[:, :128], entering) + early[:, 128:]).astype(bf16)
+            enter.append(dot_ff(before[p][:, :128], start_state[p][:, 128:]) + before[p][:, 128:])
+            seconds.append(dot_ff(pair[p][:, :128], enter[p]) + pair[p][:, 128:])
             tail = [dot_ff(reader[p][:, :128], after[p][:, i * 128 : (i + 1) * 128]) for i in range(2)]
-            read = dot_ff(tail[0], second) + tail[1] + reader[p][:, 128:]
-            seconds.append(second)
+            read = dot_ff(tail[0], seconds[p]) + tail[1] + reader[p][:, 128:]
             reads.append(read[0:1])
-        state_swap.start()
         read = jnp.concatenate(reads, axis=0) + own_write
         normed = read * lax.rsqrt(jnp.mean(read * read, axis=-1, keepdims=True) + norm_eps) * gain[...] * out_gate
         partial = dot(normed.astype(bf16), wo[...])
         for t in range(NT):
             parts_out[t] = partial[:, t * 128 : (t + 1) * 128]
 
-        def send_part(d, carry):
-            other = lax.rem(mine + d, NT)
+        steps = [(dy, dx) for dy in range(NY) for dx in range(NX) if dy or dx]
+        steps.sort(key=lambda s: -min(s[0], NY - s[0]) - min(s[1], NX - s[1]))
+        for i, (dy, dx) in enumerate(steps):
+            yy, xx = ring(y, dy, NY), ring(x, dx, NX)
             pltpu.make_async_remote_copy(
-                src_ref=parts_out.at[other], dst_ref=parts_in.at[d - 1], send_sem=part_send, recv_sem=part_recv,
-                device_id={"y": other // NX, "x": lax.rem(other, NX)}, device_id_type=MESH,
+                src_ref=parts_out.at[slot(yy, xx)], dst_ref=parts_in.at[i], send_sem=part_send, recv_sem=part_recv,
+                device_id={"y": yy, "x": xx}, device_id_type=MESH,
             ).start()
-            return carry
-
-        lax.fori_loop(1, NT, send_part, 0)
+        for p in both_prompts:
+            early = other_map[p]
+            state_out[p] = (dot_bf(early[:, :128], enter[p]) + early[:, 128:].astype(f32)).astype(bf16)
+        state_swap.start()
         for p in both_prompts:
             cache_ref[p] = seconds[p].astype(bf16)
         total = parts_out[mine]
@@ -518,8 +524,8 @@
             pltpu.VMEM((ROWS, 256), f32),
             pltpu.VMEM((ROWS, 16), f32),
             pltpu.VMEM((2, 528), f32),
-            pltpu.VMEM((2, 128, 256), f32),
-            pltpu.VMEM((2, 128, 256), f32),
+            pltpu.VMEM((2, 128, 256), bf16),
+            pltpu.VMEM((2, 128, 256), bf16),
             pltpu.VMEM((NZ, 2, 128, 256), bf16),
             pltpu.VMEM((2, 128, 128), bf16),
             pltpu.VMEM((2, 128, 128), bf16),

time: 78.8 us -> 78.1 us (level)
  no operation moved by 1% of the time
where the time goes in v3:
time: 78.1 us; the launch traced here: 77.9 us
  Pallas kernels  75.3 us (96%)
  local copies, waits for them, and re-layouts  1.99 us (3%)
    pallas_call x1, Pallas kernels, body(): pl.pallas_call(kernel, out_shape=(jax.ShapeDtypeStruct((2, HEAD, HEAD), b...  75.3 us
    unnamed x4, local copies, waits for them, and re-layouts  1.99 us

profile of v3, /device:TPU:1, one launch (start us, length us, event | category | flops | bytes accessed | tf_op | source)
XLA Modules:
  0.0 77.9 jit_solution(16951042477365614059)
XLA Ops:
  0.6 75.3 %shard_map.131 = (bf16[2,128,128]{2,1,0:T(8,128)(2,1)}, bf16[2,128]{1,0:T(2,128)(2,1)}) custom-call(bf16[512,128]{1,0:T(8,128)(2,1)} %bitcast.11, bf16[2,4096]{1,0:T(2,128)(2,1)} %fg_hbm.1, bf16[4096,128]{1,0:T(8,128)(2,1)} %wk_hbm.1, bf16[4096,128]{1,0:T(8,128)(2,1)} %wv_hbm.1, bf16[4096,128]{1,0:T(8,128)(2,1)} %wq_hbm.1, bf16[4096,128]{1,0:T(8,128)(2,1)} %wz_hbm.1, ...), custom_call_target="tpu_custom_call" | custom-call | tf_op jit(solution)/shard_map/pallas_call | solution.py:508
  75.9 0.0 copy-start
  75.9 1.5 %copy.17 = bf16[2,1,1,128,128]{4,3,2,1,0:T(8,128)(2,1)} copy(bf16[2,1,1,128,128]{4,3,2,1,0:T(8,128)(2,1)} %bitcast.12) | data formatting | bytes 131072
  77.4 0.0 copy-done
  77.4 0.5 copy.18
Async XLA Ops:
  75.9 1.5 %copy-start = (bf16[2,128]{1,0:T(2,128)(2,1)S(1)}, bf16[2,128]{1,0:T(2,128)(2,1)}, u32[]{:S(2)}) copy-start(bf16[2,128]{1,0:T(2,128)(2,1)} %get-tuple-element.11) | copy-start | bytes 1540
